TPU v7x, 32 devices: a whole 2x2x4 slice. The times are simulated.
32 devices in a mesh: fs: 16 (over z, y, x), tp: 2 (over core).
Axes of the slice: x: 2, y: 2, z: 4, core: 2. Of those that a mesh axis runs over, the one named last changes fastest.
Arguments:
- tokens: bfloat16 [12288, 2048], P('fs'), may hold values from -6 to 6
- norm_gain: float32 [2048], replicated, may hold values from 0.1 to 1.9
- up_weight: float32 [2048, 8192], P('fs', 'tp'), may hold values from -0.125 to 0.125
- up_scale: float32 [8192], P('tp'), may hold values from 0.5 to 2
- down_weight: float32 [8192, 2048], P('tp', 'fs'), may hold values from -0.0625 to 0.0625
- down_scale: float32 [2048], P('fs'), may hold values from 0.5 to 2
Outputs:
- output: bfloat16 [12288, 2048], P('fs', 'tp')
All inputs are finite; a program needn't handle non-finite values.
Results may differ from a plain program's by a relative error of at most 0.015.
Values may be sent and summed in bfloat16 or wider, within the bound.
A program may use at most 128 MiB of HBM per device.

v0:
```python
import jax
import jax.numpy as jnp
from jax import lax
from jax.sharding import PartitionSpec as P

epsilon = 1e-06


def local(tokens, norm_gain, up_weight, up_scale, down_weight, down_scale):
    floats = tokens.astype(jnp.float32)
    inverse = lax.rsqrt(jnp.mean(floats * floats, axis=-1, keepdims=True) + epsilon)
    normed = (floats * inverse * norm_gain).astype(jnp.bfloat16)
    up_half = up_weight.astype(jnp.bfloat16)
    down_half = down_weight.astype(jnp.bfloat16)
    up_pre = jnp.dot(
        normed,
        lax.all_gather(up_half, "fs", axis=0, tiled=True),
        preferred_element_type=jnp.float32,
    )
    down_whole, scale_whole = (
        lax.all_gather(down_half, "fs", axis=1, tiled=True),
        lax.all_gather(down_scale.astype(jnp.bfloat16), "fs", axis=0, tiled=True).astype(
            down_scale.dtype
        ),
    )
    hidden = jnp.square(jax.nn.relu(up_pre * up_scale)).astype(jnp.bfloat16)
    partial_value = jnp.dot(hidden, down_whole, preferred_element_type=jnp.float32).astype(
        jnp.bfloat16
    )
    summed = lax.psum_scatter(
        partial_value.astype(jnp.float32).astype(jnp.bfloat16),
        "tp",
        scatter_dimension=1,
        tiled=True,
    ).astype(jnp.float32)
    own_width = summed.shape[1]
    own_scale = lax.dynamic_slice_in_dim(
        scale_whole, lax.axis_index("tp") * own_width, own_width, 0
    )
    return (summed * own_scale).astype(jnp.bfloat16)


def solution(mesh):
    in_specs = (P("fs", None), P(), P("fs", "tp"), P("tp"), P("tp", "fs"), P("fs"))
    out_specs = P("fs", "tp")
    return jax.shard_map(local, mesh=mesh, in_specs=in_specs, out_specs=out_specs, check_vma=False)
```

profile of v0, /device:TPU:0, one launch (start us, length us, event | category | flops | bytes accessed | tf_op | source)
XLA Modules:
  0.0 539.5 jit_solution(17070823121638339327)
XLA Ops:
  6.5 0.0 copy-start
  6.5 0.0 copy-start.1
  6.5 0.0 copy-start.2
  6.5 0.0 all-gather.6.cloned.1.call-start
  6.5 2.8 convert_element_type.36
  9.4 0.0 all-gather.6.cloned.1.call-update
  9.4 0.0 all-gather.4.cloned.1.call-start
  9.4 2.7 convert_element_type.34
  12.1 0.0 all-gather.4.cloned.1.call-update
  12.2 0.0 reduce-scatter.2.cloned.1.call-start
  12.2 0.0 copy-done
  12.2 0.7 fusion
  12.9 0.0 copy-start.3
  12.9 249.0 %all-gather.6.cloned.1.call-done = bf16[4096,2048]{1,0:T(8,128)(2,1)} async-done(((bf16[4096,128]{1,0:T(8,128)(2,1)}), bf16[4096,2048]{1,0:T(8,128)(2,1)}) %all-gather.6.cloned.1.call-update) | async-done | bytes 16777232 | tf_op jit(solution)/shard_map/all_gather | solution.py:21
  261.9 192.0 %all-gather.4.cloned.1.call-done = bf16[2048,4096]{1,0:T(8,128)(2,1)} async-done(((bf16[128,4096]{1,0:T(8,128)(2,1)}), bf16[2048,4096]{1,0:T(8,128)(2,1)}) %all-gather.4.cloned.1.call-update) | async-done | bytes 16777232 | tf_op jit(solution)/shard_map/all_gather | solution.py:17
  453.9 0.0 copy-done.1
  453.9 0.0 copy-done.2
  453.9 38.2 %convolution_convert_fusion = bf16[768,2048]{1,0:T(8,128)(2,1)} fusion(bf16[4096,2048]{1,0:T(8,128)(2,1)} %all-gather.6.cloned.1.call-done, bf16[2048,4096]{1,0:T(8,128)(2,1)} %all-gather.4.cloned.1.call-done, f32[4096]{0:T(1024)S(1)} %copy-done.1, bf16[768,2048]{1,0:T(8,128)(2,1)S(1)} %copy-done, f32[2048]{0:T(1024)S(1)} %copy-done.2, ...), kind=kOutput, calls=%fused_computation.6 | convolution fusion | flops 25790251008 | bytes 39873536 | tf_op jit(solution)/shard_map/dot_general | solution.py:27
  492.1 0.0 reduce-scatter.2.cloned.1.call-update
  492.2 0.0 copy-done.3
  492.2 37.8 %all-gather = bf16[16,1,128]{2,1,0:T(2,128)(2,1)S(1)} all-gather(bf16[1,1,128]{2,1,0:T(2,128)(2,1)S(1)} %convert_bitcast_fusion), channel_id=1, replica_groups=mesh['fs'=16,'tp'=2] {'fs'}, dimensions={0}, use_global_device_ids=true | all-gather | bytes 4352 | tf_op jit(solution)/shard_map/all_gather | solution.py:22
  530.0 0.0 reduce-scatter.2.cloned.1.call-done
  530.0 3.0 multiply_convert_fusion.1
  (4 shorter events, 0.0 us)
Async XLA Ops:
  6.5 5.7 %copy-start = (bf16[768,2048]{1,0:T(8,128)(2,1)S(1)}, bf16[768,2048]{1,0:T(8,128)(2,1)}, u32[]{:S(2)}) copy-start(bf16[768,2048]{1,0:T(8,128)(2,1)} %param.6) | copy-start | bytes 9437188
  6.5 447.4 %copy-start.1 = (f32[4096]{0:T(1024)S(1)}, f32[4096]{0:T(1024)}, u32[]{:S(2)}) copy-start(f32[4096]{0:T(1024)} %param.9) | copy-start | bytes 49156
  6.5 447.4 %copy-start.2 = (f32[2048]{0:T(1024)S(1)}, f32[2048]{0:T(1024)}, u32[]{:S(2)}) copy-start(f32[2048]{0:T(1024)} %param.7) | copy-start | bytes 24580
  6.5 255.4 %all-gather.6.cloned.1.call-start = ((), (), s32[]{:S(2)}) async-start(), calls=%async_computation.2 | async-start | bytes 17825792 | tf_op jit(solution)/shard_map/all_gather | solution.py:21
  9.4 444.5 %all-gather.4.cloned.1.call-start = ((), (), s32[]{:S(2)}) async-start(), calls=%async_computation.1 | async-start | bytes 17825792 | tf_op jit(solution)/shard_map/all_gather | solution.py:17
  12.2 517.9 %reduce-scatter.2.cloned.1.call-start = ((), (), s32[]{:S(2)}) async-start(), calls=%async_computation.3 | async-start | bytes 4718592 | tf_op jit(solution)/shard_map/reduce_scatter | solution.py:30
  12.9 479.3 %copy-start.3 = (f32[128]{0:T(128)S(1)}, f32[128]{0:T(128)}, u32[]{:S(2)}) copy-start(f32[128]{0:T(128)} %param.11) | copy-start | bytes 1540
Sparse Core Ops, SparseCore 0:
  10.0 251.8 all-gather.5
  264.7 189.1 all-gather.3
  492.3 9.1 reduce-scatter.1
where the time goes:
time: 540 us
  waiting for transfers between devices  441 us (82%)
  matrix products  38.2 us (7%)
  blocking collectives  37.8 us (7%)
  between operations  13.2 us (2%)
  other arithmetic  9.18 us (2%)
    all_gather x1, waiting for transfers between devices, local(): lax.all_gather(down_half, 'fs', axis=1, tiled=True)  249 us
    all_gather x1, waiting for transfers between devices, local(): lax.all_gather(up_half, 'fs', axis=0, tiled=True)  192 us
    dot_general x1, matrix products, local(): jnp.dot(hidden, down_whole, preferred_element_type=jnp.float32)  38.2 us
    all_gather x1, blocking collectives, local(): lax.all_gather(down_scale.astype(jnp.bfloat16), 'fs', axis=0, tiled=True)  37.8 us
  transfers between devices with their start and end apart: 3, of which 2 were waited for; matrix products, arithmetic and copies ran while one was open for 1% of the time, Pallas kernels for 0%

commit v1 on v0

--- a/solution.py
+++ b/solution.py
@@ -18,7 +18,7 @@
         preferred_element_type=jnp.float32,
     )
     down_whole, scale_whole = (
-        lax.all_gather(down_half, "fs", axis=1, tiled=True),
+        jnp.concatenate(jax.lax.all_gather(down_half, "fs"), axis=1),
         lax.all_gather(down_scale.astype(jnp.bfloat16), "fs", axis=0, tiled=True).astype(
             down_scale.dtype
         ),

time: 540 us -> 482 us (0.89)
  waiting for transfers between devices: 441 us -> 362 us
  local copies, waits for them, and re-layouts: 0.03 us -> 21 us
    all_gather x1, waiting for transfers between devices: 249 us -> 191 us  [local(): jax.lax.all_gather(down_half, 'fs')]
    all_gather x1, waiting for transfers between devices: 192 us -> 171 us  [local(): lax.all_gather(up_half, 'fs', axis=0, tiled=True)]
    reshape x0 -> x1, local copies, waits for them, and re-layouts: none -> 21 us  [local(): jnp.concatenate(jax.lax.all_gather(down_half, 'fs'), axis=1)]
    dot_general x1, matrix products: 38.2 us -> 19.8 us  [local(): jnp.dot(hidden, down_whole, preferred_element_type=jnp.float32)]
    dot_general x0 -> x1, matrix products: none -> 18.5 us  [local(): jnp.dot(normed, lax.all_gather(up_half, 'fs', axis=0, tiled=True), prefer...]
  transfers between devices with their start and end apart: 3 -> 3, of which waited for: 2 -> 2; matrix products, arithmetic and copies ran while one was open for 1% -> 5% of each run, Pallas kernels for 0% -> 0%
where the time goes in v1:
time: 482 us; the launch traced here: 481 us
  waiting for transfers between devices  362 us (75%)
  matrix products  38.2 us (8%)
  blocking collectives  37.8 us (8%)
  local copies, waits for them, and re-layouts  21 us (4%)
  between operations  13.2 us (3%)
  other arithmetic  9.17 us (2%)
    all_gather x1, waiting for transfers between devices, local(): jax.lax.all_gather(down_half, 'fs')  191 us
    all_gather x1, waiting for transfers between devices, local(): lax.all_gather(up_half, 'fs', axis=0, tiled=True)  171 us
    all_gather x1, blocking collectives, local(): lax.all_gather(down_scale.astype(jnp.bfloat16), 'fs', axis=0, tiled=True)  37.8 us
    reshape x1, local copies, waits for them, and re-layouts, local(): jnp.concatenate(jax.lax.all_gather(down_half, 'fs'), axis=1)  21 us
    dot_general x1, matrix products, local(): jnp.dot(hidden, down_whole, preferred_element_type=jnp.float32)  19.8 us
    dot_general x1, matrix products, local(): jnp.dot(normed, lax.all_gather(up_half, 'fs', axis=0, tiled=True), prefer...  18.5 us
  transfers between devices with their start and end apart: 3, of which 2 were waited for; matrix products, arithmetic and copies ran while one was open for 5% of the time, Pallas kernels for 0%

profile of v1, /device:TPU:0, one launch (start us, length us, event | category | flops | bytes accessed | tf_op | source)
XLA Modules:
  0.0 481.4 jit_solution(6446146386558332321)
XLA Ops:
  6.5 0.0 copy-start
  6.5 0.0 all-gather.7.cloned.1.call-start
  6.5 2.8 convert_element_type.36
  9.4 0.0 all-gather.7.cloned.1.call-update
  9.4 0.0 all-gather.5.cloned.1.call-start
  9.4 2.7 convert_element_type.34
  12.1 0.0 all-gather.5.cloned.1.call-update
  12.1 0.0 reduce-scatter.2.cloned.1.call-start
  12.2 0.0 copy-done
  12.2 0.7 fusion
  12.9 191.0 %all-gather.7.cloned.1.call-done = bf16[65536,128]{1,0:T(8,128)(2,1)} async-done(((bf16[4096,128]{1,0:T(8,128)(2,1)}), bf16[65536,128]{1,0:T(8,128)(2,1)}) %all-gather.7.cloned.1.call-update) | async-done | bytes 16777232 | tf_op jit(solution)/shard_map/all_gather | solution.py:21
  203.9 0.0 copy-start.1
  203.9 0.0 copy-start.2
  203.9 21.0 %copy.8 = bf16[4096,16,128]{0,2,1:T(8,128)(2,1)} copy(bf16[4096,16,128]{2,0,1:T(8,128)(2,1)} %bitcast.22) | data formatting | bytes 33554432 | tf_op jit(solution)/shard_map/reshape | solution.py:21
  224.9 171.0 %all-gather.5.cloned.1.call-done = bf16[2048,4096]{1,0:T(8,128)(2,1)} async-done(((bf16[128,4096]{1,0:T(8,128)(2,1)}), bf16[2048,4096]{1,0:T(8,128)(2,1)}) %all-gather.5.cloned.1.call-update) | async-done | bytes 16777232 | tf_op jit(solution)/shard_map/all_gather | solution.py:17
  395.8 0.0 copy-done.1
  395.8 0.0 copy-done.2
  395.8 18.5 %fusion.26 = bf16[768,4096]{1,0:T(8,128)(2,1)} fusion(f32[4096]{0:T(1024)S(1)} %copy-done.1, bf16[2048,4096]{1,0:T(8,128)(2,1)} %all-gather.5.cloned.1.call-done, bf16[768,2048]{1,0:T(8,128)(2,1)S(1)} %copy-done, f32[2048]{0:T(1024)S(1)} %copy-done.2, f32[768]{0:T(1024)S(1)} %add_rsqrt_fusion), kind=kOutput, calls=%bitcast_fusion.clone.1 | convolution fusion | flops 12903776256 | bytes 26242048 | tf_op jit(solution)/shard_map/dot_general | solution.py:15
  414.3 0.0 copy-start.3
  414.3 19.8 %convolution_convert_fusion = bf16[768,2048]{1,0:T(8,128)(2,1)} fusion(bf16[4096,2048]{0,1:T(8,128)(2,1)} %bitcast.23, bf16[768,4096]{1,0:T(8,128)(2,1)} %fusion.26), kind=kOutput, calls=%fused_computation.6 | convolution fusion | flops 12886474752 | bytes 26214400 | tf_op jit(solution)/shard_map/dot_general | solution.py:27
  434.1 0.0 reduce-scatter.2.cloned.1.call-update
  434.1 0.0 copy-done.3
  434.1 37.8 %all-gather.1 = bf16[16,1,128]{2,1,0:T(2,128)(2,1)S(1)} all-gather(bf16[1,1,128]{2,1,0:T(2,128)(2,1)S(1)} %convert_bitcast_fusion), channel_id=1, replica_groups=mesh['fs'=16,'tp'=2] {'fs'}, dimensions={0}, use_global_device_ids=true | all-gather | bytes 4352 | tf_op jit(solution)/shard_map/all_gather | solution.py:22
  471.9 0.0 reduce-scatter.2.cloned.1.call-done
  471.9 3.0 multiply_convert_fusion.1
  (4 shorter events, 0.0 us)
Async XLA Ops:
  6.5 5.7 %copy-start = (bf16[768,2048]{1,0:T(8,128)(2,1)S(1)}, bf16[768,2048]{1,0:T(8,128)(2,1)}, u32[]{:S(2)}) copy-start(bf16[768,2048]{1,0:T(8,128)(2,1)} %param.6) | copy-start | bytes 9437188
  6.5 197.3 %all-gather.7.cloned.1.call-start = ((), (), s32[]{:S(2)}) async-start(), calls=%async_computation.3 | async-start | bytes 17825792 | tf_op jit(solution)/shard_map/all_gather | solution.py:21
  9.4 386.5 %all-gather.5.cloned.1.call-start = ((), (), s32[]{:S(2)}) async-start(), calls=%async_computation.1 | async-start | bytes 17825792 | tf_op jit(solution)/shard_map/all_gather | solution.py:17
  12.1 459.8 %reduce-scatter.2.cloned.1.call-start = ((), (), s32[]{:S(2)}) async-start(), calls=%async_computation.2 | async-start | bytes 4718592 | tf_op jit(solution)/shard_map/reduce_scatter | solution.py:30
  203.9 192.0 %copy-start.1 = (f32[4096]{0:T(1024)S(1)}, f32[4096]{0:T(1024)}, u32[]{:S(2)}) copy-start(f32[4096]{0:T(1024)} %param.9) | copy-start | bytes 49156
  203.9 192.0 %copy-start.2 = (f32[2048]{0:T(1024)S(1)}, f32[2048]{0:T(1024)}, u32[]{:S(2)}) copy-start(f32[2048]{0:T(1024)} %param.7) | copy-start | bytes 24580
  414.3 19.8 %copy-start.3 = (f32[128]{0:T(128)S(1)}, f32[128]{0:T(128)}, u32[]{:S(2)}) copy-start(f32[128]{0:T(128)} %param.11) | copy-start | bytes 1540
Sparse Core Ops, SparseCore 0:
  10.1 193.7 all-gather.6
  206.6 189.1 all-gather.4
  434.2 9.1 reduce-scatter.1
